TPU v7x, 256 devices: a whole 4x4x8 slice. The times are simulated.
256 devices in a mesh: sp: 64 (over z, x, core), tp: 4 (over y).
Axes of the slice: x: 4, y: 4, z: 8, core: 2. Of those that a mesh axis runs over, the one named last changes fastest.
Arguments:
- inputs: bfloat16 [32768, 2048], P('sp', 'tp'), may hold values from -45 to 45
- norm_gain: float32 [3, 2048], replicated, may hold values from 0.1 to 1.9
- w_value: bfloat16 [3, 2048, 1024], P(None, 'sp', 'tp'), may hold values from -0.125 to 0.125
- w_gate: bfloat16 [3, 2048, 1024], P(None, 'sp', 'tp'), may hold values from -0.125 to 0.125
- conv_taps: float32 [3, 31, 1024], P(None, None, 'tp'), may hold values from -5 to 5
- ln_gain: float32 [3, 1024], P(None, 'tp'), may hold values from 0.1 to 1.9
- ln_bias: float32 [3, 1024], P(None, 'tp'), may hold values from -3 to 3
- w_out: bfloat16 [3, 1024, 2048], P(None, 'tp', 'sp'), may hold values from -0.1875 to 0.1875
Outputs:
- stream: bfloat16 [32768, 2048], P('sp', 'tp')
All inputs are finite; a program needn't handle non-finite values.
Results may differ from a plain program's by a relative error of at most 0.01.
Values may be sent and summed in bfloat16 or wider, within the bound.
No kernel may reach another device: no remote copies, remote signals or barrier semaphores. Data moves between devices by JAX's collectives and lax.ppermute only.
A program may use at most 64 MiB of HBM per device.

v0:
```python
import jax
import jax.numpy as jnp
from jax import lax
from jax.sharding import PartitionSpec as P


def turned_gather(arrays, axis, dims):
    turned = [jnp.moveaxis(a, dim, 0) for a, dim in zip(arrays, dims)]
    both = jnp.concatenate([t.reshape(len(t), -1) for t in turned], axis=1)
    out, at, gathered = (lax.all_gather(both, axis, axis=0, tiled=True), 0, [])
    for t, dim in zip(turned, dims):
        piece = out[:, at : at + t[0].size].reshape(-1, *t.shape[1:])
        gathered.append(jnp.moveaxis(piece, 0, dim))
        at += t[0].size
    return tuple(gathered)


def laid_out(blocks, dim):
    blocks = jnp.moveaxis(blocks, 0, dim)
    dims = blocks.shape
    return blocks.reshape(*dims[:dim], dims[dim] * dims[dim + 1], *dims[dim + 2 :])


def copy_for_each(array, axis):
    count = lax.axis_size(axis)
    return lax.all_to_all(
        jnp.broadcast_to(array[None], (count, *array.shape)), axis, 0, 0, tiled=True
    )


def collect(array, axis, dim):
    return laid_out(copy_for_each(array, axis), dim)


def from_behind(block, axis, distance):
    devices = range(lax.axis_size(axis))
    route = [(i - distance, i) for i in devices if i - distance in devices]
    return lax.ppermute(block, axis, route)


def taken_together(array, axis):
    return copy_for_each(array, axis).sum(axis=0)


def packed_total(arrays, axis):
    ends = [0]
    for a in arrays:
        ends.append(ends[-1] + a.size)
    so_far = taken_together(jnp.concatenate([a.ravel() for a in arrays]), axis)
    return tuple((so_far[b:e].reshape(a.shape) for a, b, e in zip(arrays, ends, ends[1:])))


def cut_along(array, dim, count):
    dims = array.shape
    blocks = array.reshape(*dims[:dim], count, dims[dim] // count, *dims[dim + 1 :])
    return jnp.moveaxis(blocks, dim, 0)


def sent_and_summed(array, axis, dim):
    count = lax.axis_size(axis)
    blocks = lax.all_to_all(cut_along(array, dim, count), axis, 0, 0, tiled=True)
    return jnp.sum(blocks.astype(jnp.float32), axis=0)


def shards(inputs, norm_gain, w_value, w_gate, conv_taps, ln_gain, ln_bias, w_out):
    rows = inputs.shape[0]
    reach = conv_taps.shape[1] - 1
    layers = conv_taps.shape[0]
    channels = conv_taps.shape[2] * lax.axis_size("tp")
    whole_value, whole_gate, whole_out = turned_gather((w_value, w_gate, w_out), "sp", (1, 1, 2))
    stream = inputs
    for layer in range(layers):
        full_rows = collect(stream, "tp", 1)
        xf = full_rows.astype(jnp.float32)
        meansq = jnp.mean(xf * xf, axis=1, keepdims=True)
        hidden = (xf * lax.rsqrt(meansq + 1e-06) * norm_gain[layer][None, :]).astype(jnp.bfloat16)
        value = jnp.dot(hidden, whole_value[layer], preferred_element_type=jnp.float32)
        gate = jnp.dot(hidden, whole_gate[layer], preferred_element_type=jnp.float32)
        glu = (value * jax.nn.sigmoid(gate)).astype(jnp.bfloat16)
        rim = from_behind(glu[rows - reach :], "sp", 1)
        padded = jnp.concatenate([rim, glu], axis=0)
        count = padded.shape[0] - reach
        filtered = jnp.zeros((count, glu.shape[1]), jnp.float32)
        for tap in range(reach + 1):
            filtered = filtered + conv_taps[layer, tap][None, :] * padded[tap : tap + count].astype(
                jnp.float32
            )
        total_sum, total_sq = packed_total(
            (jnp.sum(filtered, axis=1), jnp.sum(filtered * filtered, axis=1)), "tp"
        )
        mean_val = (total_sum / channels)[:, None]
        var_val = (total_sq / channels)[:, None] - mean_val * mean_val
        normed = jax.nn.silu(
            (filtered - mean_val) * lax.rsqrt(var_val + 1e-06) * ln_gain[layer][None, :]
            + ln_bias[layer][None, :]
        ).astype(jnp.bfloat16)
        partial_out = jnp.dot(normed, whole_out[layer], preferred_element_type=jnp.float32)
        summed = sent_and_summed(partial_out.astype(jnp.bfloat16), "tp", 1)
        kept = stream.astype(jnp.float32)
        stream = (kept + summed).astype(jnp.bfloat16)
    return stream


def solution(mesh):
    in_specs = (
        P("sp", "tp"),
        P(),
        P(None, "sp", "tp"),
        P(None, "sp", "tp"),
        P(None, None, "tp"),
        P(None, "tp"),
        P(None, "tp"),
        P(None, "tp", "sp"),
    )
    out_specs = P("sp", "tp")
    return jax.shard_map(shards, mesh=mesh, in_specs=in_specs, out_specs=out_specs, check_vma=False)
```

profile of v0, /device:TPU:4, one launch (start us, length us, event | category | flops | bytes accessed | tf_op | source)
XLA Modules:
  0.0 334.8 jit_solution(13739559751142840529)
XLA Ops:
  12.4 4.5 %all-to-all-start = ((bf16[4,512,512]{1,2,0:T(8,128)(2,1)}), bf16[4,512,512]{1,2,0:T(8,128)(2,1)S(1)}, u32[]{:S(2)}, u32[]{:S(2)}) async-start(bf16[4,512,512]{1,2,0:T(8,128)(2,1)} %broadcast_in_dim.12), calls=%async_computation | async-start | bytes 4194304 | tf_op jit(solution)/shard_map/all_to_all | solution.py:26
  17.0 26.2 %all-to-all-done = bf16[4,512,512]{1,2,0:T(8,128)(2,1)S(1)} async-done(((bf16[4,512,512]{1,2,0:T(8,128)(2,1)}), bf16[4,512,512]{1,2,0:T(8,128)(2,1)S(1)}, u32[]{:S(2)}, u32[]{:S(2)}) %all-to-all-start) | async-done | bytes 2097184 | tf_op jit(solution)/shard_map/all_to_all | solution.py:26
  45.6 50.0 %all-gather.2.cloned.1.call-done = bf16[2048,2304]{1,0:T(8,128)(2,1)} async-done(((bf16[32,2304]{1,0:T(8,128)(2,1)}), bf16[2048,2304]{1,0:T(8,128)(2,1)}) %all-gather.2.cloned.1.call-update) | async-done | bytes 9437200 | tf_op jit(solution)/shard_map/all_gather | solution.py:10
  95.6 6.1 %fusion.129 = (bf16[2048,768]{1,0:T(8,128)(2,1)}, bf16[2048,768]{1,0:T(8,128)(2,1)S(1)}, bf16[2048,768]{1,0:T(8,128)(2,1)}) fusion(bf16[2048,2304]{1,0:T(8,128)(2,1)} %all-gather.2.cloned.1.call-done), kind=kLoop, calls=%fused_computation.292 | loop fusion | bytes 18874368 | tf_op jit(solution)/shard_map/slice | solution.py:12
  101.6 4.8 %copy.66 = bf16[2048,768]{0,1:T(8,128)(2,1)} copy(bf16[2048,768]{1,0:T(8,128)(2,1)} %get-tuple-element.19) | data formatting | bytes 6291456 | tf_op jit(solution)/shard_map/slice | solution.py:12
  106.4 4.7 %copy.64 = bf16[2048,768]{0,1:T(8,128)(2,1)} copy(bf16[2048,768]{1,0:T(8,128)(2,1)} %get-tuple-element.17) | data formatting | bytes 6291456 | tf_op jit(solution)/shard_map/slice | solution.py:12
  111.1 2.8 fusion.17
  115.9 2.2 collective-permute-start
  118.1 2.9 collective-permute-done
  121.0 3.0 fusion.128
  124.6 4.3 %all-to-all-start.1 = ((f32[4,1,1024]{2,1,0:T(1,128)}), f32[4,1,1024]{2,1,0:T(1,128)S(1)}, u32[]{:S(2)}, u32[]{:S(2)}) async-start(f32[4,1,1024]{2,1,0:T(1,128)} %broadcast_in_dim.13), calls=%async_computation.1 | async-start | bytes 32768 | tf_op jit(solution)/shard_map/all_to_all | solution.py:26
  128.9 3.0 copy.69
  131.9 2.4 all-to-all-done.1
  134.3 2.2 convolution_convert_fusion.2
  136.7 27.0 %all_to_all.48 = bf16[4,512,512]{2,1,0:T(8,128)(2,1)S(1)} all-to-all(bf16[4,512,512]{2,1,0:T(8,128)(2,1)S(1)} %bitcast.186), channel_id=1, replica_groups=mesh['sp'=64,'tp'=4] {'tp'}, dimensions={0} | all-to-all | bytes 4194304 | tf_op jit(solution)/shard_map/all_to_all | solution.py:61
  165.9 3.6 %all-to-all-start.3 = ((bf16[4,512,512]{1,2,0:T(8,128)(2,1)}), bf16[4,512,512]{1,2,0:T(8,128)(2,1)S(1)}, u32[]{:S(2)}, u32[]{:S(2)}) async-start(bf16[4,512,512]{1,2,0:T(8,128)(2,1)} %broadcast_in_dim.14), calls=%async_computation.3 | async-start | bytes 4194304 | tf_op jit(solution)/shard_map/all_to_all | solution.py:26
  169.6 23.2 %all-to-all-done.3 = bf16[4,512,512]{1,2,0:T(8,128)(2,1)S(1)} async-done(((bf16[4,512,512]{1,2,0:T(8,128)(2,1)}), bf16[4,512,512]{1,2,0:T(8,128)(2,1)S(1)}, u32[]{:S(2)}, u32[]{:S(2)}) %all-to-all-start.3) | async-done | bytes 2097184 | tf_op jit(solution)/shard_map/all_to_all | solution.py:26
  193.8 2.0 fusion.14
  197.8 2.1 collective-permute-start.1
  200.0 2.9 collective-permute-done.1
  202.9 2.4 fusion.127
  205.4 7.7 %all_to_all.49 = f32[4,1,1024]{2,1,0:T(1,128)S(1)} all-to-all(f32[4,1,1024]{2,1,0:T(1,128)S(1)} %broadcast_in_dim.15), channel_id=1, replica_groups=mesh['sp'=64,'tp'=4] {'tp'}, dimensions={0} | all-to-all | bytes 32768 | tf_op jit(solution)/shard_map/all_to_all | solution.py:26
  213.1 2.0 convolution_convert_fusion.1
  215.3 29.3 %all_to_all.50 = bf16[4,512,512]{2,1,0:T(8,128)(2,1)S(1)} all-to-all(bf16[4,512,512]{2,1,0:T(8,128)(2,1)S(1)} %bitcast.187), channel_id=1, replica_groups=mesh['sp'=64,'tp'=4] {'tp'}, dimensions={0} | all-to-all | bytes 4194304 | tf_op jit(solution)/shard_map/all_to_all | solution.py:61
  246.9 3.6 %all-to-all-start.6 = ((bf16[4,512,512]{1,2,0:T(8,128)(2,1)}), bf16[4,512,512]{1,2,0:T(8,128)(2,1)S(1)}, u32[]{:S(2)}, u32[]{:S(2)}) async-start(bf16[4,512,512]{1,2,0:T(8,128)(2,1)} %broadcast_in_dim.16), calls=%async_computation.6 | async-start | bytes 4194304 | tf_op jit(solution)/shard_map/all_to_all | solution.py:26
  250.5 27.4 %all-to-all-done.6 = bf16[4,512,512]{1,2,0:T(8,128)(2,1)S(1)} async-done(((bf16[4,512,512]{1,2,0:T(8,128)(2,1)}), bf16[4,512,512]{1,2,0:T(8,128)(2,1)S(1)}, u32[]{:S(2)}, u32[]{:S(2)}) %all-to-all-start.6) | async-done | bytes 2097184 | tf_op jit(solution)/shard_map/all_to_all | solution.py:26
  279.0 2.0 fusion.11
  285.0 3.1 collective-permute-done.2
  288.1 2.4 fusion.126
  290.5 7.7 %all_to_all.51 = f32[4,1,1024]{2,1,0:T(1,128)S(1)} all-to-all(f32[4,1,1024]{2,1,0:T(1,128)S(1)} %broadcast_in_dim.17), channel_id=1, replica_groups=mesh['sp'=64,'tp'=4] {'tp'}, dimensions={0} | all-to-all | bytes 32768 | tf_op jit(solution)/shard_map/all_to_all | solution.py:26
  298.3 2.0 convolution_convert_fusion
  300.5 26.1 %all_to_all.52 = bf16[4,512,512]{2,1,0:T(8,128)(2,1)S(1)} all-to-all(bf16[4,512,512]{2,1,0:T(8,128)(2,1)S(1)} %bitcast.188), channel_id=1, replica_groups=mesh['sp'=64,'tp'=4] {'tp'}, dimensions={0} | all-to-all | bytes 4194304 | tf_op jit(solution)/shard_map/all_to_all | solution.py:61
  (72 shorter events, 25.4 us)
Async XLA Ops:
  6.5 89.0 %all-gather.2.cloned.1.call-start = ((), (), s32[]{:S(2)}) async-start(), calls=%async_computation.9 | async-start | bytes 9584640 | tf_op jit(solution)/shard_map/all_gather | solution.py:10
  10.9 6.0 %copy-start.3 = (f32[3,2048]{1,0:T(4,128)S(1)}, f32[3,2048]{1,0:T(4,128)}, u32[]{:S(2)}) copy-start(f32[3,2048]{1,0:T(4,128)} %param.9) | copy-start | bytes 73732
  10.9 6.0 %copy-start.2 = (f32[3,31,256]{2,1,0:T(8,128)S(1)}, f32[3,31,256]{2,1,0:T(8,128)}, u32[]{:S(2)}) copy-start(f32[3,31,256]{2,1,0:T(8,128)} %param.12) | copy-start | bytes 285700
  12.4 30.8 %all-to-all-start = ((bf16[4,512,512]{1,2,0:T(8,128)(2,1)}), bf16[4,512,512]{1,2,0:T(8,128)(2,1)S(1)}, u32[]{:S(2)}, u32[]{:S(2)}) async-start(bf16[4,512,512]{1,2,0:T(8,128)(2,1)} %broadcast_in_dim.12), calls=%async_computation | async-start | bytes 4194304 | tf_op jit(solution)/shard_map/all_to_all | solution.py:26
  111.1 2.8 copy-start
  113.9 4.2 %copy-start.4 = (f32[3,256]{1,0:T(4,128)S(1)}, f32[3,256]{1,0:T(4,128)}, u32[]{:S(2)}) copy-start(f32[3,256]{1,0:T(4,128)} %param.14) | copy-start | bytes 9220
  113.9 15.0 %copy-start.5 = (f32[3,256]{1,0:T(4,128)S(1)}, f32[3,256]{1,0:T(4,128)}, u32[]{:S(2)}) copy-start(f32[3,256]{1,0:T(4,128)} %param.13) | copy-start | bytes 9220
  115.9 5.1 %collective-permute-start = (bf16[30,256]{1,0:T(8,128)(2,1)S(1)}, bf16[30,256]{1,0:T(8,128)(2,1)S(1)}, u32[]{:S(2)}, u32[]{:S(2)}) collective-permute-start(bf16[30,256]{1,0:T(8,128)(2,1)S(1)} %slice.856), channel_id=1, source_target_pairs={{0,4},{4,8},{8,12},{12,16},{16,20},{20,24},{24,28},{28,32},{32,36}... | collective-permute-start | bytes 46088 | tf_op jit(solution)/shard_map/ppermute | solution.py:38
  124.6 9.6 %all-to-all-start.1 = ((f32[4,1,1024]{2,1,0:T(1,128)}), f32[4,1,1024]{2,1,0:T(1,128)S(1)}, u32[]{:S(2)}, u32[]{:S(2)}) async-start(f32[4,1,1024]{2,1,0:T(1,128)} %broadcast_in_dim.13), calls=%async_computation.1 | async-start | bytes 32768 | tf_op jit(solution)/shard_map/all_to_all | solution.py:26
  136.7 27.3 %copy-start.1 = (bf16[512,512]{1,0:T(8,128)(2,1)S(1)}, bf16[512,512]{1,0:T(8,128)(2,1)}, u32[]{:S(2)}) copy-start(bf16[512,512]{1,0:T(8,128)(2,1)} %param.8) | copy-start | bytes 1572868
  165.9 26.8 %all-to-all-start.3 = ((bf16[4,512,512]{1,2,0:T(8,128)(2,1)}), bf16[4,512,512]{1,2,0:T(8,128)(2,1)S(1)}, u32[]{:S(2)}, u32[]{:S(2)}) async-start(bf16[4,512,512]{1,2,0:T(8,128)(2,1)} %broadcast_in_dim.14), calls=%async_computation.3 | async-start | bytes 4194304 | tf_op jit(solution)/shard_map/all_to_all | solution.py:26
  197.8 5.1 %collective-permute-start.1 = (bf16[30,256]{1,0:T(8,128)(2,1)S(1)}, bf16[30,256]{1,0:T(8,128)(2,1)S(1)}, u32[]{:S(2)}, u32[]{:S(2)}) collective-permute-start(bf16[30,256]{1,0:T(8,128)(2,1)S(1)} %slice.919), channel_id=1, source_target_pairs={{0,4},{4,8},{8,12},{12,16},{16,20},{20,24},{24,28},{28,32},{32,36}... | collective-permute-start | bytes 46088 | tf_op jit(solution)/shard_map/ppermute | solution.py:38
  246.9 31.1 %all-to-all-start.6 = ((bf16[4,512,512]{1,2,0:T(8,128)(2,1)}), bf16[4,512,512]{1,2,0:T(8,128)(2,1)S(1)}, u32[]{:S(2)}, u32[]{:S(2)}) async-start(bf16[4,512,512]{1,2,0:T(8,128)(2,1)} %broadcast_in_dim.16), calls=%async_computation.6 | async-start | bytes 4194304 | tf_op jit(solution)/shard_map/all_to_all | solution.py:26
  283.0 5.1 %collective-permute-start.2 = (bf16[30,256]{1,0:T(8,128)(2,1)S(1)}, bf16[30,256]{1,0:T(8,128)(2,1)S(1)}, u32[]{:S(2)}, u32[]{:S(2)}) collective-permute-start(bf16[30,256]{1,0:T(8,128)(2,1)S(1)} %slice.981), channel_id=1, source_target_pairs={{0,4},{4,8},{8,12},{12,16},{16,20},{20,24},{24,28},{28,32},{32,36}... | collective-permute-start | bytes 46088 | tf_op jit(solution)/shard_map/ppermute | solution.py:38
Sparse Core Ops, SparseCore 0:
  10.1 85.4 all-gather.1
where the time goes:
time: 336 us; the launch traced here: 335 us
  waiting for transfers between devices  138 us (41%)
  blocking collectives  97.9 us (29%)
  local copies, waits for them, and re-layouts  28.5 us (8%)
  starting transfers between devices  22.1 us (7%)
  matrix products  19.1 us (6%)
  other arithmetic  15.3 us (5%)
  between operations  13.8 us (4%)
    all_to_all x3, blocking collectives, sent_and_summed(): lax.all_to_all(cut_along(array, dim, count), axis, 0, 0, tiled=True)  82.5 us
    all_to_all x4, waiting for transfers between devices, copy_for_each(): lax.all_to_all(jnp.broadcast_to(array[None], (count, *array.shape)), axis...  79.2 us
    all_gather x1, waiting for transfers between devices, turned_gather(): out, at, gathered = (lax.all_gather(both, axis, axis=0, tiled=True), 0, [])  50 us
    slice x4, local copies, waits for them, and re-layouts, turned_gather(): piece = out[:, at:at + t[0].size].reshape(-1, *t.shape[1:])  18.5 us
    all_to_all x4, starting transfers between devices, copy_for_each(): lax.all_to_all(jnp.broadcast_to(array[None], (count, *array.shape)), axis...  16 us
    all_to_all x2, blocking collectives, copy_for_each(): lax.all_to_all(jnp.broadcast_to(array[None], (count, *array.shape)), axis...  15.4 us
    ppermute x3, waiting for transfers between devices, from_behind(): return lax.ppermute(block, axis, route)  8.89 us
    reduce_sum x3, other arithmetic, shards(): jnp.sum(filtered, axis=1)  7.83 us
  transfers between devices with their start and end apart: 8, of which 8 were waited for; matrix products, arithmetic and copies ran while one was open for 2% of the time, Pallas kernels for 0%

commit v1 on v0

--- a/solution.py
+++ b/solution.py
@@ -7,7 +7,13 @@
 def turned_gather(arrays, axis, dims):
     turned = [jnp.moveaxis(a, dim, 0) for a, dim in zip(arrays, dims)]
     both = jnp.concatenate([t.reshape(len(t), -1) for t in turned], axis=1)
-    out, at, gathered = (lax.all_gather(both, axis, axis=0, tiled=True), 0, [])
+    out, at, gathered = (
+        jnp.concatenate(
+            lax.all_to_all(jnp.stack([both] * lax.axis_size(axis)), axis, 0, 0), axis=0
+        ),
+        0,
+        [],
+    )
     for t, dim in zip(turned, dims):
         piece = out[:, at : at + t[0].size].reshape(-1, *t.shape[1:])
         gathered.append(jnp.moveaxis(piece, 0, dim))

time: 336 us -> 491 us (1.46)
  waiting for transfers between devices: 138 us -> 291 us
  between operations: 13.8 us -> 0.51 us
  starting transfers between devices: 22.1 us -> 34.1 us
    all_to_all x0 -> x1, waiting for transfers between devices: none -> 204 us  [turned_gather(): lax.all_to_all(jnp.stack([both] * lax.axis_size(axis)), axis, 0, 0)]
    all_gather x1 -> x0, waiting for transfers between devices: 50 us -> none  [turned_gather(): out, at, gathered = (lax.all_gather(both, axis, axis=0, tiled=True), 0, [])]
    all_to_all x0 -> x1, starting transfers between devices: none -> 12.3 us  [turned_gather(): lax.all_to_all(jnp.stack([both] * lax.axis_size(axis)), axis, 0, 0)]
  transfers between devices with their start and end apart: 8 -> 8, of which waited for: 8 -> 8; matrix products, arithmetic and copies ran while one was open for 2% -> 1% of each run, Pallas kernels for 0% -> 0%
where the time goes in v1:
time: 491 us; the launch traced here: 488 us
  waiting for transfers between devices  291 us (59%)
  blocking collectives  97.8 us (20%)
  starting transfers between devices  34.1 us (7%)
  local copies, waits for them, and re-layouts  31 us (6%)
  matrix products  19.1 us (4%)
  other arithmetic  14.7 us (3%)
    all_to_all x1, waiting for transfers between devices, turned_gather(): lax.all_to_all(jnp.stack([both] * lax.axis_size(axis)), axis, 0, 0)  204 us
    all_to_all x3, blocking collectives, sent_and_summed(): lax.all_to_all(cut_along(array, dim, count), axis, 0, 0, tiled=True)  82.4 us
    all_to_all x4, waiting for transfers between devices, copy_for_each(): lax.all_to_all(jnp.broadcast_to(array[None], (count, *array.shape)), axis...  78.8 us
    slice x4, local copies, waits for them, and re-layouts, turned_gather(): piece = out[:, at:at + t[0].size].reshape(-1, *t.shape[1:])  18.5 us
    all_to_all x2, blocking collectives, copy_for_each(): lax.all_to_all(jnp.broadcast_to(array[None], (count, *array.shape)), axis...  15.4 us
    all_to_all x4, starting transfers between devices, copy_for_each(): lax.all_to_all(jnp.broadcast_to(array[None], (count, *array.shape)), axis...  15.1 us
    all_to_all x1, starting transfers between devices, turned_gather(): lax.all_to_all(jnp.stack([both] * lax.axis_size(axis)), axis, 0, 0)  12.3 us
  transfers between devices with their start and end apart: 8, of which 8 were waited for; matrix products, arithmetic and copies ran while one was open for 1% of the time, Pallas kernels for 0%

profile of v1, /device:TPU:4, one launch (start us, length us, event | category | flops | bytes accessed | tf_op | source)
XLA Modules:
  0.0 488.0 jit_solution(9441938155531404696)
XLA Ops:
  2.8 4.5 all-to-all-start
  7.3 26.3 %all-to-all-done = bf16[4,512,512]{1,2,0:T(8,128)(2,1)S(1)} async-done(((bf16[4,512,512]{1,2,0:T(8,128)(2,1)}), bf16[4,512,512]{1,2,0:T(8,128)(2,1)S(1)}, u32[]{:S(2)}, u32[]{:S(2)}) %all-to-all-start) | async-done | bytes 2097184 | tf_op jit(solution)/shard_map/all_to_all | solution.py:32
  33.6 4.8 stack.2
  38.4 12.3 %all-to-all-start.1 = ((bf16[64,32,2304]{2,1,0:T(8,128)(2,1)}), bf16[64,32,2304]{2,1,0:T(8,128)(2,1)}, u32[]{:S(2)}, u32[]{:S(2)}) async-start(bf16[64,32,2304]{2,1,0:T(8,128)(2,1)} %stack.2), calls=%async_computation.1 | async-start | bytes 18874368 | tf_op jit(solution)/shard_map/all_to_all | solution.py:12
  53.2 203.7 %all-to-all-done.1 = bf16[64,32,2304]{2,1,0:T(8,128)(2,1)} async-done(((bf16[64,32,2304]{2,1,0:T(8,128)(2,1)}), bf16[64,32,2304]{2,1,0:T(8,128)(2,1)}, u32[]{:S(2)}, u32[]{:S(2)}) %all-to-all-start.1) | async-done | bytes 9437216 | tf_op jit(solution)/shard_map/all_to_all | solution.py:12
  256.9 6.1 %fusion.129 = (bf16[2048,768]{1,0:T(8,128)(2,1)}, bf16[2048,768]{1,0:T(8,128)(2,1)S(1)}, bf16[2048,768]{1,0:T(8,128)(2,1)}) fusion(bf16[2048,2304]{1,0:T(8,128)(2,1)} %bitcast.6), kind=kLoop, calls=%fused_computation.292 | loop fusion | bytes 18874368 | tf_op jit(solution)/shard_map/slice | solution.py:18
  263.0 4.8 copy.79
  267.7 4.7 copy.77
  272.4 2.8 fusion.17
  279.2 3.1 collective-permute-done
  282.3 3.0 fusion.128
  285.9 3.2 all-to-all-start.2
  289.2 3.0 copy.82
  292.2 2.3 all-to-all-done.2
  294.6 2.2 convolution_convert_fusion.2
  297.0 27.4 %all_to_all.53 = bf16[4,512,512]{2,1,0:T(8,128)(2,1)S(1)} all-to-all(bf16[4,512,512]{2,1,0:T(8,128)(2,1)S(1)} %bitcast.187), channel_id=1, replica_groups=mesh['sp'=64,'tp'=4] {'tp'}, dimensions={0} | all-to-all | bytes 4194304 | tf_op jit(solution)/shard_map/all_to_all | solution.py:67
  326.6 3.8 all-to-all-start.4
  330.4 23.7 %all-to-all-done.4 = bf16[4,512,512]{1,2,0:T(8,128)(2,1)S(1)} async-done(((bf16[4,512,512]{1,2,0:T(8,128)(2,1)}), bf16[4,512,512]{1,2,0:T(8,128)(2,1)S(1)}, u32[]{:S(2)}, u32[]{:S(2)}) %all-to-all-start.4) | async-done | bytes 2097184 | tf_op jit(solution)/shard_map/all_to_all | solution.py:32
  355.2 2.0 fusion.14
  361.2 3.1 collective-permute-done.1
  364.3 2.4 fusion.127
  366.7 7.7 %all_to_all.54 = f32[4,1,1024]{2,1,0:T(1,128)S(1)} all-to-all(f32[4,1,1024]{2,1,0:T(1,128)S(1)} %broadcast_in_dim.15), channel_id=1, replica_groups=mesh['sp'=64,'tp'=4] {'tp'}, dimensions={0} | all-to-all | bytes 32768 | tf_op jit(solution)/shard_map/all_to_all | solution.py:32
  374.5 2.0 convolution_convert_fusion.1
  376.7 27.9 %all_to_all.55 = bf16[4,512,512]{2,1,0:T(8,128)(2,1)S(1)} all-to-all(bf16[4,512,512]{2,1,0:T(8,128)(2,1)S(1)} %bitcast.188), channel_id=1, replica_groups=mesh['sp'=64,'tp'=4] {'tp'}, dimensions={0} | all-to-all | bytes 4194304 | tf_op jit(solution)/shard_map/all_to_all | solution.py:67
  406.8 3.6 all-to-all-start.7
  410.4 26.5 %all-to-all-done.7 = bf16[4,512,512]{1,2,0:T(8,128)(2,1)S(1)} async-done(((bf16[4,512,512]{1,2,0:T(8,128)(2,1)}), bf16[4,512,512]{1,2,0:T(8,128)(2,1)S(1)}, u32[]{:S(2)}, u32[]{:S(2)}) %all-to-all-start.7) | async-done | bytes 2097184 | tf_op jit(solution)/shard_map/all_to_all | solution.py:32
  442.1 2.9 collective-permute-start.2
  445.0 2.1 collective-permute-done.2
  447.2 2.4 fusion.126
  449.6 7.7 %all_to_all.56 = f32[4,1,1024]{2,1,0:T(1,128)S(1)} all-to-all(f32[4,1,1024]{2,1,0:T(1,128)S(1)} %broadcast_in_dim.17), channel_id=1, replica_groups=mesh['sp'=64,'tp'=4] {'tp'}, dimensions={0} | all-to-all | bytes 32768 | tf_op jit(solution)/shard_map/all_to_all | solution.py:32
  457.4 2.0 convolution_convert_fusion
  459.6 27.1 %all_to_all.57 = bf16[4,512,512]{2,1,0:T(8,128)(2,1)S(1)} all-to-all(bf16[4,512,512]{2,1,0:T(8,128)(2,1)S(1)} %bitcast.189), channel_id=1, replica_groups=mesh['sp'=64,'tp'=4] {'tp'}, dimensions={0} | all-to-all | bytes 4194304 | tf_op jit(solution)/shard_map/all_to_all | solution.py:67
  (78 shorter events, 26.3 us)
Async XLA Ops:
  1.3 6.0 %copy-start.3 = (bf16[3,256,32]{1,2,0:T(8,128)(2,1)S(1)}, bf16[3,256,32]{1,2,0:T(8,128)(2,1)}, u32[]{:S(2)}) copy-start(bf16[3,256,32]{1,2,0:T(8,128)(2,1)} %param.15) | copy-start | bytes 147460
  1.3 6.0 %copy-start.4 = (bf16[3,32,256]{2,1,0:T(8,128)(2,1)S(1)}, bf16[3,32,256]{2,1,0:T(8,128)(2,1)}, u32[]{:S(2)}) copy-start(bf16[3,32,256]{2,1,0:T(8,128)(2,1)} %param.11) | copy-start | bytes 147460
  1.3 6.0 %copy-start.5 = (bf16[3,32,256]{2,1,0:T(8,128)(2,1)S(1)}, bf16[3,32,256]{2,1,0:T(8,128)(2,1)}, u32[]{:S(2)}) copy-start(bf16[3,32,256]{2,1,0:T(8,128)(2,1)} %param.10) | copy-start | bytes 147460
  2.8 30.8 %all-to-all-start = ((bf16[4,512,512]{1,2,0:T(8,128)(2,1)}), bf16[4,512,512]{1,2,0:T(8,128)(2,1)S(1)}, u32[]{:S(2)}, u32[]{:S(2)}) async-start(bf16[4,512,512]{1,2,0:T(8,128)(2,1)} %broadcast_in_dim.12), calls=%async_computation | async-start | bytes 4194304 | tf_op jit(solution)/shard_map/all_to_all | solution.py:32
  38.4 12.3 %copy-start.6 = (f32[3,2048]{1,0:T(4,128)S(1)}, f32[3,2048]{1,0:T(4,128)}, u32[]{:S(2)}) copy-start(f32[3,2048]{1,0:T(4,128)} %param.9) | copy-start | bytes 73732
  38.4 12.4 %copy-start.2 = (f32[3,31,256]{2,1,0:T(8,128)S(1)}, f32[3,31,256]{2,1,0:T(8,128)}, u32[]{:S(2)}) copy-start(f32[3,31,256]{2,1,0:T(8,128)} %param.12) | copy-start | bytes 285700
  38.4 218.5 %all-to-all-start.1 = ((bf16[64,32,2304]{2,1,0:T(8,128)(2,1)}), bf16[64,32,2304]{2,1,0:T(8,128)(2,1)}, u32[]{:S(2)}, u32[]{:S(2)}) async-start(bf16[64,32,2304]{2,1,0:T(8,128)(2,1)} %stack.2), calls=%async_computation.1 | async-start | bytes 18874368 | tf_op jit(solution)/shard_map/all_to_all | solution.py:12
  272.4 2.8 copy-start
  275.2 4.0 copy-start.7
  275.2 14.0 %copy-start.8 = (f32[3,256]{1,0:T(4,128)S(1)}, f32[3,256]{1,0:T(4,128)}, u32[]{:S(2)}) copy-start(f32[3,256]{1,0:T(4,128)} %param.13) | copy-start | bytes 9220
  277.3 5.1 %collective-permute-start = (bf16[30,256]{1,0:T(8,128)(2,1)S(1)}, bf16[30,256]{1,0:T(8,128)(2,1)S(1)}, u32[]{:S(2)}, u32[]{:S(2)}) collective-permute-start(bf16[30,256]{1,0:T(8,128)(2,1)S(1)} %slice.856), channel_id=1, source_target_pairs={{0,4},{4,8},{8,12},{12,16},{16,20},{20,24},{24,28},{28,32},{32,36}... | collective-permute-start | bytes 46088 | tf_op jit(solution)/shard_map/ppermute | solution.py:44
  285.9 8.6 %all-to-all-start.2 = ((f32[4,1,1024]{2,1,0:T(1,128)}), f32[4,1,1024]{2,1,0:T(1,128)S(1)}, u32[]{:S(2)}, u32[]{:S(2)}) async-start(f32[4,1,1024]{2,1,0:T(1,128)} %broadcast_in_dim.13), calls=%async_computation.2 | async-start | bytes 32768 | tf_op jit(solution)/shard_map/all_to_all | solution.py:32
  297.0 27.7 %copy-start.1 = (bf16[512,512]{1,0:T(8,128)(2,1)S(1)}, bf16[512,512]{1,0:T(8,128)(2,1)}, u32[]{:S(2)}) copy-start(bf16[512,512]{1,0:T(8,128)(2,1)} %param.8) | copy-start | bytes 1572868
  326.6 27.5 %all-to-all-start.4 = ((bf16[4,512,512]{1,2,0:T(8,128)(2,1)}), bf16[4,512,512]{1,2,0:T(8,128)(2,1)S(1)}, u32[]{:S(2)}, u32[]{:S(2)}) async-start(bf16[4,512,512]{1,2,0:T(8,128)(2,1)} %broadcast_in_dim.14), calls=%async_computation.4 | async-start | bytes 4194304 | tf_op jit(solution)/shard_map/all_to_all | solution.py:32
  359.2 5.1 %collective-permute-start.1 = (bf16[30,256]{1,0:T(8,128)(2,1)S(1)}, bf16[30,256]{1,0:T(8,128)(2,1)S(1)}, u32[]{:S(2)}, u32[]{:S(2)}) collective-permute-start(bf16[30,256]{1,0:T(8,128)(2,1)S(1)} %slice.919), channel_id=1, source_target_pairs={{0,4},{4,8},{8,12},{12,16},{16,20},{20,24},{24,28},{28,32},{32,36}... | collective-permute-start | bytes 46088 | tf_op jit(solution)/shard_map/ppermute | solution.py:44
  406.8 30.2 %all-to-all-start.7 = ((bf16[4,512,512]{1,2,0:T(8,128)(2,1)}), bf16[4,512,512]{1,2,0:T(8,128)(2,1)S(1)}, u32[]{:S(2)}, u32[]{:S(2)}) async-start(bf16[4,512,512]{1,2,0:T(8,128)(2,1)} %broadcast_in_dim.16), calls=%async_computation.7 | async-start | bytes 4194304 | tf_op jit(solution)/shard_map/all_to_all | solution.py:32
  442.1 5.1 %collective-permute-start.2 = (bf16[30,256]{1,0:T(8,128)(2,1)S(1)}, bf16[30,256]{1,0:T(8,128)(2,1)S(1)}, u32[]{:S(2)}, u32[]{:S(2)}) collective-permute-start(bf16[30,256]{1,0:T(8,128)(2,1)S(1)} %slice.981), channel_id=1, source_target_pairs={{0,4},{4,8},{8,12},{12,16},{16,20},{20,24},{24,28},{28,32},{32,36}... | collective-permute-start | bytes 46088 | tf_op jit(solution)/shard_map/ppermute | solution.py:44
